TPU v7x, 32 devices: a whole 2x2x4 slice. The times are simulated.
32 devices in a mesh: ep: 8 (over z, y), tp: 4 (over x, core).
Axes of the slice: x: 2, y: 2, z: 4, core: 2. Of those that a mesh axis runs over, the one named last changes fastest.
Arguments:
- mixer_input: bfloat16 [4096, 2048], P('ep'), may hold values from -6 to 6
- mixer_gain: bfloat16 [2048], replicated, may hold values from 0.099609375 to 1.8984375
- pool_in: bfloat16 [2048, 1024], P(None, 'tp'), may hold values from -0.125 to 0.125
- pool_map: bfloat16 [4, 256, 256], P('tp'), may hold values from -0.375 to 0.375
- pool_scale: bfloat16 [1024], P('tp'), may hold values from 0.099609375 to 1.8984375
- pool_out: bfloat16 [1024, 2048], P('tp'), may hold values from -0.1875 to 0.1875
- expert_input: bfloat16 [3072, 2048], P('ep'), may hold values from -6 to 6
- expert_gain: bfloat16 [2048], replicated, may hold values from 0.099609375 to 1.8984375
- group_router: bfloat16 [2048, 4], replicated, may hold values from -0.125 to 0.125
- expert_router: bfloat16 [2048, 8], replicated, may hold values from -0.125 to 0.125
- routes: int32 [3072, 2], P('ep'), may hold values from 0 to 7, all different within a row; in each aligned block of 96 rows (0 to 95, 96 to 191, ...) at most 48 rows name the same one
- gate_weight: bfloat16 [8, 2048, 1024], P('ep', None, 'tp'), may hold values from -0.125 to 0.125
- up_weight: bfloat16 [8, 2048, 1024], P('ep', None, 'tp'), may hold values from -0.125 to 0.125
- down_weight: bfloat16 [8, 1024, 2048], P('ep', 'tp'), may hold values from -0.1875 to 0.1875
Outputs:
- mixer_output: bfloat16 [4096, 2048], P(('ep', 'tp'))
- expert_output: bfloat16 [3072, 2048], P(('ep', 'tp'))
Inputs may be any that keep to these rules, and one draw needn't show every extreme that they name: `routes`: each row names two different experts. In each aligned block of 96 rows no expert is named more than 48 times, a bound that some block reaches.
All inputs are finite; a program needn't handle non-finite values.
Results may differ from a plain program's by a relative error of at most 0.01.
Values may be sent and summed in bfloat16 or wider, within the bound.
A program may use at most 64 MiB of HBM per device.

v0:
```python
import jax
import jax.numpy as jnp
from jax import lax
from jax.sharding import PartitionSpec as P

RIM = 15
EPS = 1e-06


def passed_along(value, axis, steps):
    count = lax.axis_size(axis)
    leading, last = (max(0, -steps), min(count, count - steps))
    return lax.ppermute(value, axis, [(source, source + steps) for source in range(leading, last)])


def norm_rows(values, gain):
    floats = values.astype(jnp.float32)
    scale = lax.rsqrt(jnp.mean(floats * floats, axis=-1, keepdims=True) + EPS)
    return (floats * scale * gain.astype(jnp.float32)).astype(jnp.bfloat16)


def route_weights(rows, group_router, expert_router, route_rows):
    group_logits = jnp.dot(rows, group_router, preferred_element_type=jnp.float32)
    expert_logits = jnp.dot(rows, expert_router, preferred_element_type=jnp.float32)
    groups = group_logits.shape[1]
    experts = expert_logits.shape[1]
    member = (
        jnp.arange(experts, dtype=jnp.int32)[:, None] // (experts // groups)
        == jnp.arange(groups, dtype=jnp.int32)[None, :]
    ).astype(jnp.float32)
    group_exp = jnp.exp(group_logits)
    group_prob = group_exp / jnp.sum(group_exp, axis=1, keepdims=True)
    expert_exp = jnp.exp(expert_logits)
    within = jnp.dot(expert_exp, member, precision=lax.Precision.HIGHEST)
    prob = expert_exp * jnp.dot(group_prob / within, member.T, precision=lax.Precision.HIGHEST)
    chosen = (route_rows[:, :, None] == jnp.arange(experts, dtype=jnp.int32)[None, None, :]).astype(
        jnp.float32
    )
    picked = jnp.sum(chosen * prob[:, None, :], axis=2)
    return picked / jnp.sum(picked, axis=1, keepdims=True)


def mixer_half(mixer_input, mixer_gain, pool_in, pool_map, pool_scale, pool_out):
    normed = norm_rows(mixer_input, mixer_gain)
    pooled_in = jnp.dot(normed, pool_in, preferred_element_type=jnp.float32).astype(jnp.bfloat16)
    local_rows = pooled_in.shape[0]
    groups_here = pool_map.shape[0]
    channels = pool_map.shape[1]
    border = passed_along(pooled_in[local_rows - RIM :], "ep", 1)
    padded = jnp.concatenate([border, pooled_in], axis=0).astype(jnp.float32)
    padded = padded.reshape(local_rows + RIM, groups_here, channels)
    leading = lax.axis_index("tp") * groups_here
    windows = jnp.left_shift(jnp.int32(2), leading + jnp.arange(groups_here, dtype=jnp.int32))
    window_sum = jnp.zeros((local_rows, groups_here, channels), jnp.float32)
    for offset in range(RIM + 1):
        active = (offset < windows).astype(jnp.float32)
        window_sum = (
            window_sum + padded[RIM - offset : RIM - offset + local_rows] * active[None, :, None]
        )
    position = lax.axis_index("ep") * local_rows + jnp.arange(local_rows, dtype=jnp.int32)
    counts_here = jnp.minimum(position[:, None] + 1, windows[None, :]).astype(jnp.float32)
    pooled = (window_sum / counts_here[:, :, None] - padded[RIM:]).astype(jnp.bfloat16)
    mapped = jnp.einsum("tgc,gce->tge", pooled, pool_map, preferred_element_type=jnp.float32)
    mixed_rows = (
        mapped.reshape(local_rows, groups_here * channels) * pool_scale.astype(jnp.float32)
    ).astype(jnp.bfloat16)
    return lax.psum_scatter(
        jnp.dot(mixed_rows, pool_out, preferred_element_type=jnp.float32).astype(jnp.bfloat16),
        "tp",
        scatter_dimension=0,
        tiled=True,
    )


def slot_positions(route_rows, blocks, experts):
    flat = route_rows.reshape(blocks, -1)
    onehot = (flat[:, :, None] == jnp.arange(experts, dtype=jnp.int32)[None, None, :]).astype(
        jnp.int32
    )
    before = jnp.cumsum(onehot, axis=1) - onehot
    return (jnp.sum(before * onehot, axis=2), flat)


def dispatch_rows(normed, route_rows, blocks, slots_each, experts):
    block_len = normed.shape[0] // blocks
    positions, flat = slot_positions(route_rows, blocks, experts)
    block_index = jnp.arange(blocks, dtype=jnp.int32)[:, None]
    slot_index = block_index * slots_each + positions
    token_index = block_index * block_len + jnp.arange(2 * block_len, dtype=jnp.int32)[None, :] // 2
    table = jnp.full((blocks * slots_each, experts), -1, jnp.int32)
    table = table.at[slot_index.reshape(-1), flat.reshape(-1)].set(token_index.reshape(-1))
    fetched = normed[jnp.maximum(table, 0)]
    return jnp.where((table >= 0)[:, :, None], fetched, jnp.zeros_like(fetched))


def expert_half(
    expert_input,
    expert_gain,
    group_router,
    expert_router,
    routes,
    gate_weight,
    up_weight,
    down_weight,
):
    normed = norm_rows(expert_input, expert_gain)
    tp_count = lax.axis_size("tp")
    tp_place = lax.axis_index("tp")
    experts = expert_router.shape[1]
    block_len = normed.shape[0] // tp_count
    slots_each = 4 * block_len // experts
    own_rows = lax.dynamic_slice_in_dim(normed, tp_place * block_len, block_len, 0)
    own_routes = lax.dynamic_slice_in_dim(routes, tp_place * block_len, block_len, 0)
    sending = dispatch_rows(own_rows, own_routes, 1, slots_each, experts)
    arrived = lax.all_to_all(sending, "ep", split_axis=1, concat_axis=1, tiled=True)
    received = lax.all_gather(arrived, "tp", axis=0, tiled=True)
    held = gate_weight.shape[0]
    model = received.shape[2]
    portion = received
    portion = portion.reshape(lax.axis_size("tp") * slots_each, -1, held, model)
    gate = jnp.einsum("csed,edh->cseh", portion, gate_weight, preferred_element_type=jnp.float32)
    upward = jnp.einsum("csed,edh->cseh", portion, up_weight, preferred_element_type=jnp.float32)
    hidden = (jax.nn.silu(gate) * upward).astype(jnp.bfloat16)
    result = jnp.einsum("cseh,ehd->csed", hidden, down_weight, preferred_element_type=jnp.float32)
    summed = lax.psum_scatter(
        result.reshape(lax.axis_size("tp") * slots_each, -1, model).astype(jnp.bfloat16),
        "tp",
        scatter_dimension=0,
        tiled=True,
    )
    returned = lax.all_to_all(summed, "ep", split_axis=1, concat_axis=1, tiled=True)
    positions, flat = slot_positions(own_routes, 1, experts)
    lookup = positions[0] * experts + flat[0]
    picked = (
        returned.reshape(slots_each * experts, model)[lookup]
        .astype(jnp.float32)
        .reshape(block_len, 2, model)
    )
    weights = route_weights(own_rows, group_router, expert_router, own_routes)
    return jnp.sum(picked * weights[:, :, None], axis=1).astype(jnp.bfloat16)


def on_device(
    mixer_input,
    mixer_gain,
    pool_in,
    pool_map,
    pool_scale,
    pool_out,
    expert_input,
    expert_gain,
    group_router,
    expert_router,
    routes,
    gate_weight,
    up_weight,
    down_weight,
):
    mixer_output = mixer_half(mixer_input, mixer_gain, pool_in, pool_map, pool_scale, pool_out)
    expert_output = expert_half(
        expert_input,
        expert_gain,
        group_router,
        expert_router,
        routes,
        gate_weight,
        up_weight,
        down_weight,
    )
    return (mixer_output, expert_output)


def solution(mesh):
    return jax.shard_map(
        on_device,
        mesh=mesh,
        in_specs=(
            P("ep", None),
            P(),
            P(None, "tp"),
            P("tp", None, None),
            P("tp"),
            P("tp", None),
            P("ep", None),
            P(),
            P(),
            P(),
            P("ep", None),
            P("ep", None, "tp"),
            P("ep", None, "tp"),
            P("ep", "tp", None),
        ),
        out_specs=(P(("ep", "tp"), None), P(("ep", "tp"), None)),
        check_vma=False,
    )
```

profile of v0, /device:TPU:0, one launch (start us, length us, event | category | flops | bytes accessed | tf_op | source)
XLA Modules:
  0.0 257.5 jit_solution(10104831046113127895)
XLA Ops:
  7.2 0.0 all-gather.2.cloned.1.call-start
  7.2 1.9 multiply_reduce_fusion
  9.2 2.0 convert_element_type.167
  11.2 0.8 constant_dynamic-slice_fusion
  12.0 0.1 copy.34
  12.1 0.1 eq.66
  12.2 0.1 reshape_reshape.3
  12.4 0.6 reduce-window.6
  13.0 0.2 slice_reduce_fusion
  13.3 0.1 fusion.50
  13.4 9.4 %scatter_fusion = s32[48,8]{0,1:T(8,128)S(1)} fusion(s32[48,8]{0,1:T(8,128)S(1)} %broadcast_in_dim.11, s32[192]{0:T(256)S(1)} %bitcast.87, s32[192]{0:T(256)S(1)} %and_select_fusion.1), kind=kCustom, calls=%fused_computation.2 | custom fusion | bytes 3840 | tf_op jit(solution)/shard_map/scatter | solution.py:91
  22.8 0.1 dynamic-slice
  22.9 0.1 copy.36
  23.0 0.1 reshape.525
  23.1 1.3 fusion.23
  24.4 2.5 gather_fusion
  26.8 1.8 copy_select_fusion
  28.7 44.1 %all_to_all.10 = bf16[48,8,2048]{2,0,1:T(8,128)(2,1)S(1)} all-to-all(bf16[48,8,2048]{2,0,1:T(8,128)(2,1)S(1)} %copy_select_fusion), channel_id=1, replica_groups=mesh['ep'=8,'tp'=4] {'ep'}, dimensions={1} | all-to-all | bytes 3145728 | tf_op jit(solution)/shard_map/all_to_all | solution.py:115
  72.8 2.0 copy.38
  74.8 0.0 all-gather.2.cloned.1.call-update
  74.8 0.2 reduce-scatter.5.cloned.1.call-start
  75.1 45.3 %all-gather.2.cloned.1.call-done = bf16[192,8,2048]{2,1,0:T(8,128)(2,1)} async-done(((bf16[48,8,2048]{2,1,0:T(8,128)(2,1)}), bf16[192,8,2048]{2,1,0:T(8,128)(2,1)}) %all-gather.2.cloned.1.call-update) | async-done | bytes 6291472 | tf_op jit(solution)/shard_map/all_gather | solution.py:116
  120.3 5.8 %fusion.20 = f32[192,8,256]{2,1,0:T(8,128)} fusion(bf16[192,8,2048]{2,1,0:T(8,128)(2,1)} %all-gather.2.cloned.1.call-done, bf16[1,2048,256]{2,1,0:T(8,128)(2,1)S(1)} %copy-done.8), kind=kOutput, calls=%fused_computation.35 | convolution fusion | flops 1610612736 | bytes 8912896 | tf_op jit(solution)/shard_map/csed,edh->cseh/dot_general | solution.py:121
  126.1 12.2 %convolution_convert_fusion = bf16[192,8,2048]{2,1,0:T(8,128)(2,1)} fusion(bf16[192,8,2048]{2,1,0:T(8,128)(2,1)} %all-gather.2.cloned.1.call-done, f32[192,8,256]{2,1,0:T(8,128)} %fusion.20, bf16[1,256,2048]{2,1,0:T(8,128)(2,1)S(1)} %copy-done, bf16[1,2048,256]{2,1,0:T(8,128)(2,1)S(1)} %copy-done.9), kind=kOutput, calls=%fused_computation.5 | convolution fusion | flops 3226730496 | bytes 16252928 | tf_op jit(solution)/shard_map/cseh,ehd->csed/dot_general | solution.py:124
  138.4 0.0 reduce-scatter.5.cloned.1.call-update
  138.4 0.0 reduce-scatter.3.cloned.1.call-start
  138.5 0.6 copy-done.7
  139.1 0.9 copy-done.2
  140.0 0.5 fusion
  140.5 0.8 fusion.12
  141.3 0.7 copy-done.3
  142.0 3.4 %collective-permute-start = (bf16[15,256]{1,0:T(8,128)(2,1)S(1)}, bf16[15,256]{1,0:T(8,128)(2,1)S(1)}, u32[]{:S(2)}, u32[]{:S(2)}) collective-permute-start(bf16[15,256]{1,0:T(8,128)(2,1)S(1)} %slice.103), channel_id=1, source_target_pairs={{0,4},{4,8},{8,12},{12,16},{16,20},{20,24},{24,28},{1,5},{5,9},{9,... | collective-permute-start | bytes 23048 | tf_op jit(solution)/shard_map/ppermute | solution.py:13
  145.5 1.2 collective-permute-done
  146.7 1.0 maximum_convert_fusion
  147.8 4.8 %convolution_convert_fusion.1 = bf16[512,2048]{1,0:T(8,128)(2,1)} fusion(bf16[256,2048]{1,0:T(8,128)(2,1)} %param.19, f32[256]{0:T(256)S(1)} %convert_element_type.163, f32[527,256]{1,0:T(8,128)S(1)} %maximum_convert_fusion, f32[512]{0:T(512)S(1)} %minimum_convert_fusion, f32[]{:T(128)S(6)} %convert_element_type.160, f32[]{:T(128)S(6)} %convert_element_type.159, ...), kind=kOutput, calls=%fused_computation.10 | convolution fusion | flops 609746944 | bytes 11668544 | tf_op jit(solution)/shard_map/dot_general | solution.py:68
  152.6 44.8 %reduce-scatter.5.cloned.1.call-done = bf16[48,8,2048]{2,1,0:T(8,128)(2,1)} async-done(((bf16[192,8,2048]{2,1,0:T(8,128)(2,1)}), bf16[48,8,2048]{2,1,0:T(8,128)(2,1)}) %reduce-scatter.5.cloned.1.call-update) | async-done | bytes 1572880 | tf_op jit(solution)/shard_map/reduce_scatter | solution.py:125
  197.4 3.4 %copy.39 = bf16[48,8,2048]{2,0,1:T(8,128)(2,1)} copy(bf16[48,8,2048]{2,1,0:T(8,128)(2,1)} %reduce-scatter.5.cloned.1.call-done) | data formatting | bytes 3145728 | tf_op jit(solution)/shard_map/reduce_scatter | solution.py:125
  200.8 5.6 %all-to-all-start.1 = ((bf16[48,8,2048]{2,0,1:T(8,128)(2,1)}), bf16[48,8,2048]{2,0,1:T(8,128)(2,1)}, u32[]{:S(2)}, u32[]{:S(2)}) async-start(bf16[48,8,2048]{2,0,1:T(8,128)(2,1)} %copy.39), calls=%async_computation.3 | async-start | bytes 3145728 | tf_op jit(solution)/shard_map/all_to_all | solution.py:131
  206.5 0.2 fusion.55
  206.7 0.2 convolution_exponential_fusion
  206.9 0.3 fusion.16
  207.2 0.2 convolution_multiply_fusion.1
  207.5 0.1 copy.41
  207.6 35.9 %all-to-all-done.1 = bf16[48,8,2048]{2,0,1:T(8,128)(2,1)} async-done(((bf16[48,8,2048]{2,0,1:T(8,128)(2,1)}), bf16[48,8,2048]{2,0,1:T(8,128)(2,1)}, u32[]{:S(2)}, u32[]{:S(2)}) %all-to-all-start.1) | async-done | bytes 1572896 | tf_op jit(solution)/shard_map/all_to_all | solution.py:131
  243.4 2.3 copy.44
  245.7 1.1 gather_fusion.1
  246.9 1.0 reshape.522
  247.8 3.1 %multiply_reduce_fusion.1 = bf16[96,2048]{1,0:T(8,128)(2,1)} fusion(f32[96,2,2048]{2,1,0:T(2,128)S(1)} %reshape.522, f32[96,2]{1,0:T(8,128)S(1)} %copy.41), kind=kLoop, calls=%fused_computation.23 | loop fusion | flops 589824 | bytes 1966848 | tf_op jit(solution)/shard_map/reduce_sum | solution.py:140
  (45 shorter events, 0.3 us)
Async XLA Ops:
  7.2 119.0 %copy-start = (bf16[1,256,2048]{2,1,0:T(8,128)(2,1)S(1)}, bf16[1,256,2048]{2,1,0:T(8,128)(2,1)}, u32[]{:S(2)}) copy-start(bf16[1,256,2048]{2,1,0:T(8,128)(2,1)} %param.27) | copy-start | bytes 3145732
  7.2 2.0 copy-start.1
  7.2 113.1 %all-gather.2.cloned.1.call-start = ((), (), s32[]{:S(2)}) async-start(), calls=%async_computation.5 | async-start | bytes 7864320 | tf_op jit(solution)/shard_map/all_gather | solution.py:116
  11.2 11.7 %copy-start.6 = (bf16[2048]{0:T(1024)(128)(2,1)S(1)}, bf16[2048]{0:T(1024)(128)(2,1)}, u32[]{:S(2)}) copy-start(bf16[2048]{0:T(1024)(128)(2,1)} %param.21) | copy-start | bytes 12292
  74.8 45.5 %copy-start.8 = (bf16[1,2048,256]{2,1,0:T(8,128)(2,1)S(1)}, bf16[1,2048,256]{2,1,0:T(8,128)(2,1)}, u32[]{:S(2)}) copy-start(bf16[1,2048,256]{2,1,0:T(8,128)(2,1)} %param.25) | copy-start | bytes 3145732
  74.8 51.3 %copy-start.9 = (bf16[1,2048,256]{2,1,0:T(8,128)(2,1)S(1)}, bf16[1,2048,256]{2,1,0:T(8,128)(2,1)}, u32[]{:S(2)}) copy-start(bf16[1,2048,256]{2,1,0:T(8,128)(2,1)} %param.26) | copy-start | bytes 3145732
  74.8 122.6 %reduce-scatter.5.cloned.1.call-start = ((), (), s32[]{:S(2)}) async-start(), calls=%async_computation.6 | async-start | bytes 7864320 | tf_op jit(solution)/shard_map/reduce_scatter | solution.py:125
  138.4 0.7 copy-start.7
  138.4 1.6 copy-start.2
  138.4 112.6 %reduce-scatter.3.cloned.1.call-start = ((), (), s32[]{:S(2)}) async-start(), calls=%async_computation.4 | async-start | bytes 2621440 | tf_op jit(solution)/shard_map/reduce_scatter | solution.py:67
  139.1 1.4 copy-start.10
  140.5 5.0 %copy-start.11 = (bf16[256]{0:T(256)(128)(2,1)S(1)}, bf16[256]{0:T(256)(128)(2,1)}, u32[]{:S(2)}) copy-start(bf16[256]{0:T(256)(128)(2,1)} %param.18) | copy-start | bytes 1540
  141.3 0.7 copy-start.3
  142.0 4.7 %collective-permute-start = (bf16[15,256]{1,0:T(8,128)(2,1)S(1)}, bf16[15,256]{1,0:T(8,128)(2,1)S(1)}, u32[]{:S(2)}, u32[]{:S(2)}) collective-permute-start(bf16[15,256]{1,0:T(8,128)(2,1)S(1)} %slice.103), channel_id=1, source_target_pairs={{0,4},{4,8},{8,12},{12,16},{16,20},{20,24},{24,28},{1,5},{5,9},{9,... | collective-permute-start | bytes 23048 | tf_op jit(solution)/shard_map/ppermute | solution.py:13
  200.8 5.7 %copy-start.5 = (bf16[2048,4]{0,1:T(4,128)(2,1)S(1)}, bf16[2048,4]{0,1:T(4,128)(2,1)}, u32[]{:S(2)}) copy-start(bf16[2048,4]{0,1:T(4,128)(2,1)} %param.22) | copy-start | bytes 49156
  200.8 5.9 %copy-start.4 = (bf16[2048,8]{0,1:T(8,128)(2,1)S(1)}, bf16[2048,8]{0,1:T(8,128)(2,1)}, u32[]{:S(2)}) copy-start(bf16[2048,8]{0,1:T(8,128)(2,1)} %param.23) | copy-start | bytes 98308
  200.8 42.6 %all-to-all-start.1 = ((bf16[48,8,2048]{2,0,1:T(8,128)(2,1)}), bf16[48,8,2048]{2,0,1:T(8,128)(2,1)}, u32[]{:S(2)}, u32[]{:S(2)}) async-start(bf16[48,8,2048]{2,0,1:T(8,128)(2,1)} %copy.39), calls=%async_computation.3 | async-start | bytes 3145728 | tf_op jit(solution)/shard_map/all_to_all | solution.py:131
Sparse Core Ops, SparseCore 0:
  74.9 45.3 all-gather.1
  138.5 58.8 reduce-scatter.4
  200.5 31.1 reduce-scatter.2
where the time goes:
time: 258 us
  waiting for transfers between devices  127 us (49%)
  blocking collectives  44.1 us (17%)
  local copies, waits for them, and re-layouts  25.7 us (10%)
  matrix products  24.5 us (9%)
  between operations  14.1 us (5%)
  other arithmetic  12.6 us (5%)
  starting transfers between devices  9.32 us (4%)
    all_gather x1, waiting for transfers between devices, expert_half(): received = lax.all_gather(arrived, 'tp', axis=0, tiled=True)  45.3 us
    reduce_scatter x1, waiting for transfers between devices, expert_half(): lax.psum_scatter(result.reshape(lax.axis_size('tp') * slots_each, -1, mod...  44.8 us
    all_to_all x1, blocking collectives, expert_half(): lax.all_to_all(sending, 'ep', split_axis=1, concat_axis=1, tiled=True)  44.1 us
    all_to_all x1, waiting for transfers between devices, expert_half(): lax.all_to_all(summed, 'ep', split_axis=1, concat_axis=1, tiled=True)  35.9 us
    dot_general x1, matrix products, expert_half(): jnp.einsum('cseh,ehd->csed', hidden, down_weight, preferred_element_type=...  12.2 us
    scatter x1, local copies, waits for them, and re-layouts, dispatch_rows(): table.at[slot_index.reshape(-1), flat.reshape(-1)]  9.38 us
    dot_general x1, matrix products, expert_half(): jnp.einsum('csed,edh->cseh', portion, gate_weight, preferred_element_type...  5.78 us
    all_to_all x1, starting transfers between devices, expert_half(): lax.all_to_all(summed, 'ep', split_axis=1, concat_axis=1, tiled=True)  5.65 us
  transfers between devices with their start and end apart: 5, of which 4 were waited for; matrix products, arithmetic and copies ran while one was open for 7% of the time, Pallas kernels for 0%

commit v1 on v0

--- a/solution.py
+++ b/solution.py
@@ -128,7 +128,10 @@
         scatter_dimension=0,
         tiled=True,
     )
-    returned = lax.all_to_all(summed, "ep", split_axis=1, concat_axis=1, tiled=True)
+    returned = jnp.concatenate(
+        lax.all_to_all(jnp.stack(jnp.split(summed, lax.axis_size("ep"), axis=1)), "ep", 0, 0),
+        axis=1,
+    )
     positions, flat = slot_positions(own_routes, 1, experts)
     lookup = positions[0] * experts + flat[0]
     picked = (

time: 258 us -> 274 us (1.062)
  local copies, waits for them, and re-layouts: 25.7 us -> 41.7 us
    split x0 -> x1, local copies, waits for them, and re-layouts: none -> 9.73 us  [expert_half(): jnp.split(summed, lax.axis_size('ep'), axis=1)]
    unnamed x24 -> x33, local copies, waits for them, and re-layouts: 2.27 us -> 8.95 us
    reduce_scatter x1 -> x0, local copies, waits for them, and re-layouts: 3.43 us -> none  [expert_half(): lax.psum_scatter(result.reshape(lax.axis_size('tp') * slots_each, -1, mod...]
  transfers between devices with their start and end apart: 5 -> 5, of which waited for: 4 -> 4; matrix products, arithmetic and copies ran while one was open for 7% -> 12% of each run, Pallas kernels for 0% -> 0%
where the time goes in v1:
time: 274 us; the launch traced here: 273 us
  waiting for transfers between devices  127 us (46%)
  blocking collectives  44.1 us (16%)
  local copies, waits for them, and re-layouts  41.7 us (15%)
  matrix products  24.5 us (9%)
  between operations  14.1 us (5%)
  other arithmetic  12.4 us (5%)
  starting transfers between devices  9.54 us (3%)
    all_gather x1, waiting for transfers between devices, expert_half(): received = lax.all_gather(arrived, 'tp', axis=0, tiled=True)  45.3 us
    reduce_scatter x1, waiting for transfers between devices, expert_half(): lax.psum_scatter(result.reshape(lax.axis_size('tp') * slots_each, -1, mod...  44.8 us
    all_to_all x1, blocking collectives, expert_half(): lax.all_to_all(sending, 'ep', split_axis=1, concat_axis=1, tiled=True)  44.1 us
    all_to_all x1, waiting for transfers between devices, expert_half(): lax.all_to_all(jnp.stack(jnp.split(summed, lax.axis_size('ep'), axis=1)),...  35.8 us
    dot_general x1, matrix products, expert_half(): jnp.einsum('cseh,ehd->csed', hidden, down_weight, preferred_element_type=...  12.2 us
    split x1, local copies, waits for them, and re-layouts, expert_half(): jnp.split(summed, lax.axis_size('ep'), axis=1)  9.73 us
    scatter x1, local copies, waits for them, and re-layouts, dispatch_rows(): table.at[slot_index.reshape(-1), flat.reshape(-1)]  9.38 us
    unnamed x33, local copies, waits for them, and re-layouts  8.95 us
  transfers between devices with their start and end apart: 5, of which 4 were waited for; matrix products, arithmetic and copies ran while one was open for 12% of the time, Pallas kernels for 0%

profile of v1, /device:TPU:0, one launch (start us, length us, event | category | flops | bytes accessed | tf_op | source)
XLA Modules:
  0.0 273.2 jit_solution(870969157352661302)
XLA Ops:
  7.2 0.9 constant_dynamic-slice_fusion
  8.2 0.1 copy.111
  8.3 0.1 eq.66
  8.4 0.1 reshape_reshape.6
  8.5 1.8 multiply_reduce_fusion
  10.3 2.0 convert_element_type.167
  12.4 0.6 reduce-window.6
  13.0 0.2 slice_reduce_fusion
  13.4 9.4 %scatter_fusion = s32[48,8]{0,1:T(8,128)S(1)} fusion(s32[48,8]{0,1:T(8,128)S(1)} %broadcast_in_dim.11, s32[192]{0:T(256)S(1)} %bitcast.104, s32[192]{0:T(256)S(1)} %and_select_fusion.1), kind=kCustom, calls=%fused_computation.2 | custom fusion | bytes 3840 | tf_op jit(solution)/shard_map/scatter | solution.py:91
  23.1 1.3 fusion.23
  24.4 2.5 gather_fusion
  26.8 1.8 copy_select_fusion
  28.7 44.1 %all_to_all.10 = bf16[48,8,2048]{2,0,1:T(8,128)(2,1)S(1)} all-to-all(bf16[48,8,2048]{2,0,1:T(8,128)(2,1)S(1)} %copy_select_fusion), channel_id=1, replica_groups=mesh['ep'=8,'tp'=4] {'ep'}, dimensions={1} | all-to-all | bytes 3145728 | tf_op jit(solution)/shard_map/all_to_all | solution.py:115
  72.8 2.0 copy.115
  74.8 0.2 reduce-scatter.5.cloned.1.call-start
  75.0 45.3 %all-gather.2.cloned.1.call-done = bf16[192,8,2048]{2,1,0:T(8,128)(2,1)} async-done(((bf16[48,8,2048]{2,1,0:T(8,128)(2,1)}), bf16[192,8,2048]{2,1,0:T(8,128)(2,1)}) %all-gather.2.cloned.1.call-update) | async-done | bytes 6291472 | tf_op jit(solution)/shard_map/all_gather | solution.py:116
  120.3 5.8 %fusion.20 = f32[192,8,256]{2,1,0:T(8,128)} fusion(bf16[192,8,2048]{2,1,0:T(8,128)(2,1)} %all-gather.2.cloned.1.call-done, bf16[1,2048,256]{2,1,0:T(8,128)(2,1)S(1)} %copy-done.9), kind=kOutput, calls=%fused_computation.35 | convolution fusion | flops 1610612736 | bytes 8912896 | tf_op jit(solution)/shard_map/csed,edh->cseh/dot_general | solution.py:121
  126.1 12.2 %convolution_convert_fusion = bf16[192,8,2048]{2,1,0:T(8,128)(2,1)} fusion(bf16[192,8,2048]{2,1,0:T(8,128)(2,1)} %all-gather.2.cloned.1.call-done, f32[192,8,256]{2,1,0:T(8,128)} %fusion.20, bf16[1,256,2048]{2,1,0:T(8,128)(2,1)S(1)} %copy-done, bf16[1,2048,256]{2,1,0:T(8,128)(2,1)S(1)} %copy-done.10), kind=kOutput, calls=%fused_computation.5 | convolution fusion | flops 3226730496 | bytes 16252928 | tf_op jit(solution)/shard_map/cseh,ehd->csed/dot_general | solution.py:124
  138.4 0.6 copy-done.8
  139.0 0.9 copy-done.3
  140.0 0.5 fusion
  140.5 0.8 fusion.12
  141.3 0.7 copy-done.4
  142.0 3.6 %collective-permute-start = (bf16[15,256]{1,0:T(8,128)(2,1)S(1)}, bf16[15,256]{1,0:T(8,128)(2,1)S(1)}, u32[]{:S(2)}, u32[]{:S(2)}) collective-permute-start(bf16[15,256]{1,0:T(8,128)(2,1)S(1)} %slice.103), channel_id=1, source_target_pairs={{0,4},{4,8},{8,12},{12,16},{16,20},{20,24},{24,28},{1,5},{5,9},{9,... | collective-permute-start | bytes 23048 | tf_op jit(solution)/shard_map/ppermute | solution.py:13
  145.7 1.0 collective-permute-done
  146.7 1.0 maximum_convert_fusion
  147.7 4.8 %convolution_convert_fusion.1 = bf16[512,2048]{1,0:T(8,128)(2,1)} fusion(bf16[256,2048]{1,0:T(8,128)(2,1)} %param.19, f32[256]{0:T(256)S(1)} %convert_element_type.163, f32[527,256]{1,0:T(8,128)S(1)} %maximum_convert_fusion, f32[512]{0:T(512)S(1)} %minimum_convert_fusion, f32[]{:T(128)S(6)} %convert_element_type.160, f32[]{:T(128)S(6)} %convert_element_type.159, ...), kind=kOutput, calls=%fused_computation.10 | convolution fusion | flops 609746944 | bytes 11668544 | tf_op jit(solution)/shard_map/dot_general | solution.py:68
  152.6 44.8 %reduce-scatter.5.cloned.1.call-done = bf16[48,8,2048]{2,1,0:T(8,128)(2,1)} async-done(((bf16[192,8,2048]{2,1,0:T(8,128)(2,1)}), bf16[48,8,2048]{2,1,0:T(8,128)(2,1)}) %reduce-scatter.5.cloned.1.call-update) | async-done | bytes 1572880 | tf_op jit(solution)/shard_map/reduce_scatter | solution.py:125
  197.4 9.7 %fusion.55 = (bf16[48,1,2048]{2,1,0:T(2,128)(2,1)S(1)}, bf16[48,1,2048]{2,1,0:T(2,128)(2,1)S(1)}, bf16[48,1,2048]{2,1,0:T(2,128)(2,1)S(1)}, bf16[48,1,2048]{2,1,...) fusion(bf16[48,8,2048]{2,1,0:T(8,128)(2,1)} %reduce-scatter.5.c, ...), kind=kLoop, calls=%fused_computation.126 | loop fusion | bytes 3145728 | tf_op jit(solution)/shard_map/split | solution.py:132
  207.1 0.8 bitcast_dynamic-update-slice_fusion.7
  207.9 0.8 bitcast_dynamic-update-slice_fusion.6
  208.7 0.8 bitcast_dynamic-update-slice_fusion.5
  209.5 0.8 bitcast_dynamic-update-slice_fusion.4
  210.3 0.8 bitcast_dynamic-update-slice_fusion.3
  211.1 0.8 bitcast_dynamic-update-slice_fusion.2
  211.9 0.8 bitcast_dynamic-update-slice_fusion.1
  212.7 0.8 bitcast_dynamic-update-slice_fusion
  213.5 5.6 %all-to-all-start.1 = ((bf16[8,48,1,2048]{3,1,2,0:T(8,128)(2,1)}), bf16[8,48,1,2048]{3,1,2,0:T(8,128)(2,1)S(1)}, u32[]{:S(2)}, u32[]{:S(2)}) async-start(bf16[8,48,1,2048]{3,1,2,0:T(8,128)(2,1)} %bitcast_dynamic-update-slice_fusion), calls=%async_computation.3 | async-start | bytes 3145728 | tf_op jit(solution)/shard_map/all_to_all | solution.py:132
  219.1 0.2 fusion.56
  219.4 0.2 convolution_exponential_fusion
  219.6 0.3 fusion.16
  219.8 0.2 convolution_multiply_fusion.1
  220.2 35.8 %all-to-all-done.1 = bf16[8,48,1,2048]{3,1,2,0:T(8,128)(2,1)S(1)} async-done(((bf16[8,48,1,2048]{3,1,2,0:T(8,128)(2,1)}), bf16[8,48,1,2048]{3,1,2,0:T(8,128)(2,1)S(1)}, u32[]{:S(2)}, u32[]{:S(2)}) %all-to-all-start.1) | async-done | bytes 1572896 | tf_op jit(solution)/shard_map/all_to_all | solution.py:132
  256.0 1.2 copy-done.1
  257.1 2.3 copy.136
  259.4 2.0 gather_fusion.1
  261.4 2.1 reshape.522
  263.6 3.1 %multiply_reduce_fusion.1 = bf16[96,2048]{1,0:T(8,128)(2,1)} fusion(f32[96,2,2048]{2,1,0:T(2,128)S(1)} %reshape.522, f32[96,2]{1,0:T(8,128)S(1)} %copy.117), kind=kLoop, calls=%fused_computation.23 | loop fusion | flops 589824 | bytes 1966848 | tf_op jit(solution)/shard_map/reduce_sum | solution.py:143
  (55 shorter events, 0.8 us)
Async XLA Ops:
  7.2 118.9 %copy-start = (bf16[1,256,2048]{2,1,0:T(8,128)(2,1)S(1)}, bf16[1,256,2048]{2,1,0:T(8,128)(2,1)}, u32[]{:S(2)}) copy-start(bf16[1,256,2048]{2,1,0:T(8,128)(2,1)} %param.27) | copy-start | bytes 3145732
  7.2 3.2 %copy-start.2 = (bf16[384,2048]{1,0:T(8,128)(2,1)S(1)}, bf16[384,2048]{1,0:T(8,128)(2,1)}, u32[]{:S(2)}) copy-start(bf16[384,2048]{1,0:T(8,128)(2,1)} %param.20) | copy-start | bytes 4718596
  7.2 113.1 %all-gather.2.cloned.1.call-start = ((), (), s32[]{:S(2)}) async-start(), calls=%async_computation.5 | async-start | bytes 7864320 | tf_op jit(solution)/shard_map/all_gather | solution.py:116
  12.4 10.7 %copy-start.7 = (bf16[2048]{0:T(1024)(128)(2,1)S(1)}, bf16[2048]{0:T(1024)(128)(2,1)}, u32[]{:S(2)}) copy-start(bf16[2048]{0:T(1024)(128)(2,1)} %param.21) | copy-start | bytes 12292
  74.8 45.5 %copy-start.9 = (bf16[1,2048,256]{2,1,0:T(8,128)(2,1)S(1)}, bf16[1,2048,256]{2,1,0:T(8,128)(2,1)}, u32[]{:S(2)}) copy-start(bf16[1,2048,256]{2,1,0:T(8,128)(2,1)} %param.25) | copy-start | bytes 3145732
  74.8 51.3 %copy-start.10 = (bf16[1,2048,256]{2,1,0:T(8,128)(2,1)S(1)}, bf16[1,2048,256]{2,1,0:T(8,128)(2,1)}, u32[]{:S(2)}) copy-start(bf16[1,2048,256]{2,1,0:T(8,128)(2,1)} %param.26) | copy-start | bytes 3145732
  74.8 122.6 %reduce-scatter.5.cloned.1.call-start = ((), (), s32[]{:S(2)}) async-start(), calls=%async_computation.6 | async-start | bytes 7864320 | tf_op jit(solution)/shard_map/reduce_scatter | solution.py:125
  138.4 0.7 copy-start.8
  138.4 1.6 copy-start.3
  138.4 128.3 %reduce-scatter.3.cloned.1.call-start = ((), (), s32[]{:S(2)}) async-start(), calls=%async_computation.4 | async-start | bytes 2621440 | tf_op jit(solution)/shard_map/reduce_scatter | solution.py:67
  139.0 1.4 copy-start.11
  140.5 5.2 %copy-start.12 = (bf16[256]{0:T(256)(128)(2,1)S(1)}, bf16[256]{0:T(256)(128)(2,1)}, u32[]{:S(2)}) copy-start(bf16[256]{0:T(256)(128)(2,1)} %param.18) | copy-start | bytes 1540
  141.3 0.7 copy-start.4
  142.0 4.7 %collective-permute-start = (bf16[15,256]{1,0:T(8,128)(2,1)S(1)}, bf16[15,256]{1,0:T(8,128)(2,1)S(1)}, u32[]{:S(2)}, u32[]{:S(2)}) collective-permute-start(bf16[15,256]{1,0:T(8,128)(2,1)S(1)} %slice.103), channel_id=1, source_target_pairs={{0,4},{4,8},{8,12},{12,16},{16,20},{20,24},{24,28},{1,5},{5,9},{9,... | collective-permute-start | bytes 23048 | tf_op jit(solution)/shard_map/ppermute | solution.py:13
  213.5 5.7 %copy-start.6 = (bf16[2048,4]{0,1:T(4,128)(2,1)S(1)}, bf16[2048,4]{0,1:T(4,128)(2,1)}, u32[]{:S(2)}) copy-start(bf16[2048,4]{0,1:T(4,128)(2,1)} %param.22) | copy-start | bytes 49156
  213.5 5.9 %copy-start.5 = (bf16[2048,8]{0,1:T(8,128)(2,1)S(1)}, bf16[2048,8]{0,1:T(8,128)(2,1)}, u32[]{:S(2)}) copy-start(bf16[2048,8]{0,1:T(8,128)(2,1)} %param.23) | copy-start | bytes 98308
  213.5 42.5 %all-to-all-start.1 = ((bf16[8,48,1,2048]{3,1,2,0:T(8,128)(2,1)}), bf16[8,48,1,2048]{3,1,2,0:T(8,128)(2,1)S(1)}, u32[]{:S(2)}, u32[]{:S(2)}) async-start(bf16[8,48,1,2048]{3,1,2,0:T(8,128)(2,1)} %bitcast_dynamic-update-slice_fusion), calls=%async_computation.3 | async-start | bytes 3145728 | tf_op jit(solution)/shard_map/all_to_all | solution.py:132
  256.0 1.2 copy-start.1
Sparse Core Ops, SparseCore 0:
  74.9 45.3 all-gather.1
  138.5 58.8 reduce-scatter.4
  200.5 31.1 reduce-scatter.2
